TPU v7x, 32 devices: a whole 2x2x4 slice. The times are simulated.
32 devices in a mesh: ep: 8 (over z, x), tp: 4 (over y, core).
Axes of the slice: x: 2, y: 2, z: 4, core: 2. Of those that a mesh axis runs over, the one named last changes fastest.
Arguments:
- tokens: bfloat16 [2048, 2048], P('ep'), may hold values from -6 to 6
- norm_gain: float32 [2048], replicated, may hold values from 0.1 to 1.9
- expert_ids: int32 [2048, 4], P('ep'), may hold values from 0 to 7, all different within a row; in each aligned block of 256 rows (0 to 255, 256 to 511, ...) at most 256 rows name the same one
- route_weights: float32 [2048, 4], P('ep'), may hold values from 0.05 to 1
- gate_weight: bfloat16 [8, 2048, 2048], P('ep', None, 'tp'), as said below
- up_weight: bfloat16 [8, 2048, 2048], P('ep', None, 'tp'), as said below
- down_weight: bfloat16 [8, 2048, 2048], P('ep', 'tp'), may hold values from -0.125 to 0.125
Outputs:
- mixed: bfloat16 [2048, 2048], P('ep', 'tp')
Inputs may be any that keep to these rules, and one draw needn't show every extreme that they name: `expert_ids`: each row names 4 different experts. In the rows of one device no expert is named by more than 256 rows, and in every draw some expert is named by exactly 256 rows of some device. `gate_weight`: independent entries of mean zero, drawn for each expert separately. `up_weight`: independent entries of mean zero, drawn for each expert separately.
All inputs are finite; a program needn't handle non-finite values.
Results may differ from a plain program's by a relative error of at most 0.014.
Values may be sent and summed in bfloat16 or wider, within the bound.
A program may use at most 128 MiB of HBM per device.

v0:
```python
import jax
import jax.numpy as jnp
from jax import lax
from jax.sharding import PartitionSpec as P


def per_device(tokens, norm_gain, expert_ids, route_weights, gate_weight, up_weight, down_weight):
    tok_dev, width = tokens.shape
    top = expert_ids.shape[1]
    n_ep = lax.axis_size("ep")
    n_tp = lax.axis_size("tp")
    exp_dev = gate_weight.shape[0]
    experts = exp_dev * n_ep
    capacity = 2 * tok_dev * top // experts
    quarter = width // n_tp
    values = tokens.astype(jnp.float32)
    scale = lax.rsqrt(jnp.mean(values * values, axis=1, keepdims=True) + 1e-06)
    normed = (values * scale * norm_gain[None, :]).astype(jnp.bfloat16)
    flat = expert_ids.reshape(-1)
    count = flat.shape[0]
    onehot = (flat[:, None] == jnp.arange(experts, dtype=jnp.int32)[None, :]).astype(jnp.int32)
    before = jnp.cumsum(onehot, axis=0) - onehot
    slot = jnp.sum(before * onehot, axis=1)
    position = flat * capacity + slot
    source_tok = jnp.arange(count, dtype=jnp.int32) // top
    buffer_tok = jnp.zeros((experts * capacity,), jnp.int32).at[position].set(source_tok)
    buffer_live = jnp.zeros((experts * capacity,), jnp.int32).at[position].set(1)
    columns = lax.dynamic_slice_in_dim(normed, lax.axis_index("tp") * quarter, quarter, 1)
    outgoing = jnp.where(buffer_live[:, None] > 0, columns[buffer_tok], jnp.zeros((), jnp.bfloat16))
    outgoing = outgoing.reshape(n_ep, exp_dev, capacity, quarter)
    received = lax.all_gather(
        lax.all_to_all(outgoing, "ep", split_axis=0, concat_axis=0, tiled=True),
        "tp",
        axis=3,
        tiled=True,
    )
    gate = jnp.einsum("sxcd,xdf->sxcf", received, gate_weight, preferred_element_type=jnp.float32)
    upper = jnp.einsum("sxcd,xdf->sxcf", received, up_weight, preferred_element_type=jnp.float32)
    gate = jnp.minimum(gate, 7.0)
    upper = jnp.clip(upper, -7.0, 7.0)
    hidden = ((upper + 1.0) * (gate * jax.nn.sigmoid(1.702 * gate))).astype(jnp.bfloat16)
    partial_value = jnp.einsum(
        "sxcf,xfd->sxcd", hidden, down_weight, preferred_element_type=jnp.float32
    )
    rounded = partial_value.astype(jnp.bfloat16)
    summed = (
        lax.psum_scatter(rounded, "tp", scatter_dimension=3, tiled=True)
        .astype(jnp.float32)
        .astype(jnp.bfloat16)
    )
    returned = lax.all_to_all(summed, "ep", split_axis=0, concat_axis=0, tiled=True)
    returned = returned.reshape(experts * capacity, quarter)
    picked = returned[position].reshape(tok_dev, top, quarter)
    mixed = jnp.sum(route_weights[:, :, None] * picked.astype(jnp.float32), axis=1)
    return mixed.astype(jnp.bfloat16)


def solution(mesh):
    in_specs = (
        P("ep", None),
        P(),
        P("ep", None),
        P("ep", None),
        P("ep", None, "tp"),
        P("ep", None, "tp"),
        P("ep", "tp", None),
    )
    out_specs = P("ep", "tp")
    return jax.shard_map(
        per_device, mesh=mesh, in_specs=in_specs, out_specs=out_specs, check_vma=False
    )
```

profile of v0, /device:TPU:8, one launch (start us, length us, event | category | flops | bytes accessed | tf_op | source)
XLA Modules:
  0.0 313.2 jit_solution(5834554861335021660)
XLA Ops:
  6.5 3.0 convert_element_type.41
  9.5 0.3 multiply_reduce_fusion.1
  9.8 0.1 copy.15
  10.2 2.3 reduce-window.6
  12.5 0.3 slice_reduce_fusion
  12.8 0.2 reduce-window.9
  13.0 0.1 copy.14
  13.4 4.3 %scatter_custom_fusion.1 = s32[2048]{0:T(1024)S(1)} fusion(s32[1024]{0:T(1024)S(1)} %bitcast.102, s32[1024]{0:T(1024)S(1)} %add_select_fusion, s32[]{:T(128)} %constant.18.clone.1), kind=kCustom, calls=%fused_computation.45 | custom fusion | bytes 8196 | tf_op jit(solution)/shard_map/scatter | solution.py:26
  17.7 4.3 %scatter_custom_fusion = s32[2048]{0:T(1024)S(1)} fusion(s32[1024]{0:T(1024)S(1)} %bitcast.103, s32[1024]{0:T(1024)S(1)} %broadcast.124, s32[]{:T(128)} %constant.18.clone.1), kind=kCustom, calls=%fused_computation.48 | custom fusion | bytes 8196 | tf_op jit(solution)/shard_map/scatter | solution.py:27
  22.1 0.8 dynamic-slice
  22.8 1.1 fusion.24
  24.0 9.2 %gather_fusion = bf16[2048,512]{1,0:T(8,128)(2,1)} fusion(bf16[256,512]{1,0:T(8,128)(2,1)S(1)} %fusion.24, s32[2048]{0:T(1024)S(1)} %fusion.29), kind=kCustom, calls=%fused_computation | custom fusion | bytes 4202496 | tf_op jit(solution)/shard_map/gather | solution.py:29
  33.2 1.8 broadcast_select_fusion
  34.9 53.4 %all_to_all.10 = bf16[8,1,256,512]{3,2,1,0:T(8,128)(2,1)} all-to-all(bf16[8,1,256,512]{3,2,1,0:T(8,128)(2,1)S(1)} %broadcast_select_fusion), channel_id=1, replica_groups=mesh['ep'=8,'tp'=4] {'ep'}, dimensions={0} | all-to-all | bytes 4194304 | tf_op jit(solution)/shard_map/all_to_all | solution.py:32
  88.4 57.8 %all-gather.2.cloned.1.call-done = bf16[8,1,256,2048]{3,2,0,1:T(8,128)(2,1)} async-done(((bf16[8,1,256,512]{3,2,0,1:T(8,128)(2,1)}), bf16[8,1,256,2048]{3,2,0,1:T(8,128)(2,1)}) %all-gather.2.cloned.1.call-update) | async-done | bytes 8388624 | tf_op jit(solution)/shard_map/all_gather | solution.py:31
  146.3 10.4 %fusion = f32[8,256,512]{2,1,0:T(8,128)} fusion(bf16[8,1,256,2048]{3,2,0,1:T(8,128)(2,1)} %all-gather.2.cloned.1.call-done, bf16[1,2048,512]{2,1,0:T(8,128)(2,1)} %param.11), kind=kOutput, calls=%fused_computation.4 | convolution fusion | flops 4294967296 | bytes 14680064 | tf_op jit(solution)/shard_map/sxcd,xdf->sxcf/dot_general | solution.py:37
  156.7 15.2 %convert_bitcast_fusion = bf16[8,1,256,2048]{3,2,0,1:T(8,128)(2,1)} fusion(bf16[1,512,2048]{2,1,0:T(8,128)(2,1)S(1)} %copy-done, f32[8,256,512]{2,1,0:T(8,128)} %fusion, bf16[8,1,256,2048]{3,2,0,1:T(8,128)(2,1)} %all-gather.2.cloned.1.call-done, bf16[1,2048,512]{2,1,0:T(8,128)(2,1)} %param.12), kind=kOutput, calls=%fused_computation.8 | convolution fusion | flops 8604614656 | bytes 25165824 | tf_op jit(solution)/shard_map/sxcf,xfd->sxcd/dot_general | solution.py:42
  171.9 71.4 %reduce-scatter.2.cloned.1.call-done = bf16[8,1,256,512]{3,2,0,1:T(8,128)(2,1)} async-done(((bf16[8,1,256,2048]{3,2,0,1:T(8,128)(2,1)}), bf16[8,1,256,512]{3,2,0,1:T(8,128)(2,1)}) %reduce-scatter.2.cloned.1.call-update) | async-done | bytes 2097168 | tf_op jit(solution)/shard_map/reduce_scatter | solution.py:47
  243.3 6.2 %all-to-all-start.1 = ((bf16[8,1,256,512]{3,2,1,0:T(8,128)(2,1)}), bf16[8,1,256,512]{3,2,1,0:T(8,128)(2,1)}, u32[]{:S(2)}, u32[]{:S(2)}) async-start(bf16[8,1,256,512]{3,2,1,0:T(8,128)(2,1)} %bitcast.100), calls=%async_computation.2 | async-start | bytes 4194304 | tf_op jit(solution)/shard_map/all_to_all | solution.py:51
  249.5 0.1 copy.13
  249.7 45.5 %all-to-all-done.1 = bf16[8,1,256,512]{3,2,1,0:T(8,128)(2,1)} async-done(((bf16[8,1,256,512]{3,2,1,0:T(8,128)(2,1)}), bf16[8,1,256,512]{3,2,1,0:T(8,128)(2,1)}, u32[]{:S(2)}, u32[]{:S(2)}) %all-to-all-start.1) | async-done | bytes 2097184 | tf_op jit(solution)/shard_map/all_to_all | solution.py:51
  295.1 5.8 %gather_fusion.1 = bf16[1024,512]{1,0:T(8,128)(2,1)S(1)} fusion(bf16[2048,512]{1,0:T(8,128)(2,1)} %bitcast.26, s32[1024]{0:T(1024)S(1)} %broadcast_clamp_fusion), kind=kCustom, calls=%fused_computation.1 | custom fusion | bytes 2101248 | tf_op jit(solution)/shard_map/gather | solution.py:53
  301.0 1.7 reshape.116
  302.7 3.7 %multiply_reduce_fusion = bf16[256,512]{1,0:T(8,128)(2,1)} fusion(f32[256,4,512]{2,1,0:T(4,128)} %reshape.116, f32[256,4]{1,0:T(8,128)S(1)} %copy.13), kind=kLoop, calls=%fused_computation.21 | loop fusion | flops 917504 | bytes 2363392 | tf_op jit(solution)/shard_map/reduce_sum | solution.py:54
  (27 shorter events, 0.6 us)
Async XLA Ops:
  6.5 150.2 %copy-start = (bf16[1,512,2048]{2,1,0:T(8,128)(2,1)S(1)}, bf16[1,512,2048]{2,1,0:T(8,128)(2,1)}, u32[]{:S(2)}) copy-start(bf16[1,512,2048]{2,1,0:T(8,128)(2,1)} %param.13) | copy-start | bytes 6291460
  6.5 3.0 copy-start.1
  6.5 139.7 %all-gather.2.cloned.1.call-start = ((), (), s32[]{:S(2)}) async-start(), calls=%async_computation.3 | async-start | bytes 10485760 | tf_op jit(solution)/shard_map/all_gather | solution.py:31
  6.5 3.3 %copy-start.2 = (s32[256,4]{0,1:T(4,128)S(1)}, s32[256,4]{0,1:T(4,128)}, u32[]{:S(2)}) copy-start(s32[256,4]{0,1:T(4,128)} %param.9) | copy-start | bytes 12292
  88.4 154.9 %reduce-scatter.2.cloned.1.call-start = ((), (), s32[]{:S(2)}) async-start(), calls=%async_computation.4 | async-start | bytes 10485760 | tf_op jit(solution)/shard_map/reduce_scatter | solution.py:47
  243.3 6.2 %copy-start.3 = (f32[256,4]{0,1:T(4,128)S(1)}, f32[256,4]{0,1:T(4,128)}, u32[]{:S(2)}) copy-start(f32[256,4]{0,1:T(4,128)} %param.10) | copy-start | bytes 12292
  243.3 51.8 %all-to-all-start.1 = ((bf16[8,1,256,512]{3,2,1,0:T(8,128)(2,1)}), bf16[8,1,256,512]{3,2,1,0:T(8,128)(2,1)}, u32[]{:S(2)}, u32[]{:S(2)}) async-start(bf16[8,1,256,512]{3,2,1,0:T(8,128)(2,1)} %bitcast.100), calls=%async_computation.2 | async-start | bytes 4194304 | tf_op jit(solution)/shard_map/all_to_all | solution.py:51
Sparse Core Ops, SparseCore 0:
  88.5 57.7 all-gather.1
  172.1 71.2 reduce-scatter.1
where the time goes:
time: 317 us; the launch traced here: 313 us
  waiting for transfers between devices  175 us (55%)
  blocking collectives  53.4 us (17%)
  local copies, waits for them, and re-layouts  27.2 us (9%)
  matrix products  25.6 us (8%)
  between operations  13.6 us (4%)
  other arithmetic  12.4 us (4%)
  starting transfers between devices  6.22 us (2%)
    reduce_scatter x1, waiting for transfers between devices, per_device(): lax.psum_scatter(rounded, 'tp', scatter_dimension=3, tiled=True)  71.4 us
    all_gather x1, waiting for transfers between devices, per_device(): lax.all_gather(lax.all_to_all(outgoing, 'ep', split_axis=0, concat_axis=0...  57.8 us
    all_to_all x1, blocking collectives, per_device(): lax.all_to_all(outgoing, 'ep', split_axis=0, concat_axis=0, tiled=True)  53.4 us
    all_to_all x1, waiting for transfers between devices, per_device(): lax.all_to_all(summed, 'ep', split_axis=0, concat_axis=0, tiled=True)  45.5 us
    dot_general x1, matrix products, per_device(): jnp.einsum('sxcf,xfd->sxcd', hidden, down_weight, preferred_element_type=...  15.2 us
    dot_general x1, matrix products, per_device(): jnp.einsum('sxcd,xdf->sxcf', received, gate_weight, preferred_element_typ...  10.4 us
    gather x1, local copies, waits for them, and re-layouts, per_device(): columns[buffer_tok]  9.16 us
  transfers between devices with their start and end apart: 3, of which 3 were waited for; matrix products, arithmetic and copies ran while one was open for 0% of the time, Pallas kernels for 0%

commit v1 on v0

--- a/solution.py
+++ b/solution.py
@@ -4,7 +4,19 @@
 from jax.sharding import PartitionSpec as P
 
 
-def per_device(tokens, norm_gain, expert_ids, route_weights, gate_weight, up_weight, down_weight):
+def normalise(tokens, norm_gain):
+    values = tokens.astype(jnp.float32)
+    scale = lax.rsqrt(jnp.mean(values * values, axis=1, keepdims=True) + 1e-06)
+    return (values * scale * norm_gain[None, :]).astype(jnp.bfloat16)
+
+
+def activate(gate, upper):
+    gate = jnp.minimum(gate, 7.0)
+    upper = jnp.clip(upper, -7.0, 7.0)
+    return (upper + 1.0) * (gate * jax.nn.sigmoid(1.702 * gate))
+
+
+def routed(tokens, norm_gain, expert_ids, route_weights, gate_weight, up_weight, down_weight):
     tok_dev, width = tokens.shape
     top = expert_ids.shape[1]
     n_ep = lax.axis_size("ep")
@@ -13,9 +25,7 @@
     experts = exp_dev * n_ep
     capacity = 2 * tok_dev * top // experts
     quarter = width // n_tp
-    values = tokens.astype(jnp.float32)
-    scale = lax.rsqrt(jnp.mean(values * values, axis=1, keepdims=True) + 1e-06)
-    normed = (values * scale * norm_gain[None, :]).astype(jnp.bfloat16)
+    normed = normalise(tokens, norm_gain)
     flat = expert_ids.reshape(-1)
     count = flat.shape[0]
     onehot = (flat[:, None] == jnp.arange(experts, dtype=jnp.int32)[None, :]).astype(jnp.int32)
@@ -36,23 +46,52 @@
     )
     gate = jnp.einsum("sxcd,xdf->sxcf", received, gate_weight, preferred_element_type=jnp.float32)
     upper = jnp.einsum("sxcd,xdf->sxcf", received, up_weight, preferred_element_type=jnp.float32)
-    gate = jnp.minimum(gate, 7.0)
-    upper = jnp.clip(upper, -7.0, 7.0)
-    hidden = ((upper + 1.0) * (gate * jax.nn.sigmoid(1.702 * gate))).astype(jnp.bfloat16)
+    hidden = activate(gate, upper).astype(jnp.bfloat16)
     partial_value = jnp.einsum(
         "sxcf,xfd->sxcd", hidden, down_weight, preferred_element_type=jnp.float32
     )
     rounded = partial_value.astype(jnp.bfloat16)
-    summed = (
-        lax.psum_scatter(rounded, "tp", scatter_dimension=3, tiled=True)
-        .astype(jnp.float32)
-        .astype(jnp.bfloat16)
-    )
+    summed = lax.psum_scatter(rounded, "tp", scatter_dimension=3, tiled=True)
     returned = lax.all_to_all(summed, "ep", split_axis=0, concat_axis=0, tiled=True)
     returned = returned.reshape(experts * capacity, quarter)
     picked = returned[position].reshape(tok_dev, top, quarter)
     mixed = jnp.sum(route_weights[:, :, None] * picked.astype(jnp.float32), axis=1)
     return mixed.astype(jnp.bfloat16)
+
+
+def dense(tokens, norm_gain, expert_ids, route_weights, gate_weight, up_weight, down_weight):
+    tok_dev, width = tokens.shape
+    n_ep = lax.axis_size("ep")
+    n_tp = lax.axis_size("tp")
+    quarter = width // n_tp
+    mine = lax.axis_index("ep")
+    normed = normalise(tokens, norm_gain)
+    columns = lax.dynamic_slice_in_dim(normed, lax.axis_index("tp") * quarter, quarter, 1)
+    onehot = expert_ids[:, :, None] == jnp.arange(n_ep, dtype=jnp.int32)[None, None, :]
+    table = jnp.sum(jnp.where(onehot, route_weights[:, :, None], 0.0), axis=1)
+    weights = lax.all_to_all(table.T, "ep", split_axis=0, concat_axis=0, tiled=True)
+    every = lax.all_gather(columns, ("ep", "tp"), axis=0, tiled=False)
+    every = every.reshape(n_ep, n_tp, tok_dev, quarter)
+    gate_w = gate_weight.reshape(n_tp, quarter, -1)
+    up_w = up_weight.reshape(n_tp, quarter, -1)
+    gate = jnp.einsum("epcd,pdf->ecf", every, gate_w, preferred_element_type=jnp.float32)
+    upper = jnp.einsum("epcd,pdf->ecf", every, up_w, preferred_element_type=jnp.float32)
+    hidden = activate(gate, upper).astype(jnp.bfloat16)
+    down_w = down_weight[0].reshape(-1, n_tp, quarter)
+    out = jnp.einsum("ecf,fpd->epcd", hidden, down_w, preferred_element_type=jnp.float32)
+    out = jnp.where(weights[:, None, :, None] > 0, weights[:, None, :, None] * out, 0.0)
+    out = out.astype(jnp.bfloat16).reshape(n_ep * n_tp, tok_dev, quarter)
+    return lax.psum_scatter(out, ("ep", "tp"), scatter_dimension=0, tiled=False)
+
+
+def per_device(tokens, norm_gain, expert_ids, route_weights, gate_weight, up_weight, down_weight):
+    tok_dev, top = expert_ids.shape
+    experts = gate_weight.shape[0] * lax.axis_size("ep")
+    whole = gate_weight.shape[0] == 1 and 2 * tok_dev * top // experts >= tok_dev
+    form = dense if whole else routed
+    return form(
+        tokens, norm_gain, expert_ids, route_weights, gate_weight, up_weight, down_weight
+    )
 
 
 def solution(mesh):
@@ -65,7 +104,6 @@
         P("ep", None, "tp"),
         P("ep", "tp", None),
     )
-    out_specs = P("ep", "tp")
     return jax.shard_map(
-        per_device, mesh=mesh, in_specs=in_specs, out_specs=out_specs, check_vma=False
+        per_device, mesh=mesh, in_specs=in_specs, out_specs=P("ep", "tp"), check_vma=False
     )

time: 317 us -> 276 us (0.87)
  the two profiles are of different devices: /device:TPU:8 before, /device:TPU:0 now
where the time goes in v1:
time: 276 us
  waiting for transfers between devices  217 us (79%)
  matrix products  26 us (9%)
  between operations  13.4 us (5%)
  starting transfers between devices  7.32 us (3%)
  other arithmetic  6.34 us (2%)
  local copies, waits for them, and re-layouts  5.9 us (2%)
    reduce_scatter x1, waiting for transfers between devices, dense(): return lax.psum_scatter(out, ('ep', 'tp'), scatter_dimension=0, tiled=False)  149 us
    all_gather x1, waiting for transfers between devices, dense(): every = lax.all_gather(columns, ('ep', 'tp'), axis=0, tiled=False)  65.5 us
    dot_general x1, matrix products, dense(): jnp.einsum('ecf,fpd->epcd', hidden, down_w, preferred_element_type=jnp.fl...  15.5 us
    dot_general x1, matrix products, dense(): jnp.einsum('epcd,pdf->ecf', every, up_w, preferred_element_type=jnp.float32)  10.4 us
    all_to_all x1, starting transfers between devices, dense(): lax.all_to_all(table.T, 'ep', split_axis=0, concat_axis=0, tiled=True)  7.28 us
  transfers between devices with their start and end apart: 3, of which 3 were waited for; matrix products, arithmetic and copies ran while one was open for 2% of the time, Pallas kernels for 0%

profile of v1, /device:TPU:0, one launch (start us, length us, event | category | flops | bytes accessed | tf_op | source)
XLA Modules:
  0.0 275.6 jit_solution(10777329323813777890)
XLA Ops:
  6.5 0.0 copy-start
  6.5 0.0 copy-start.1
  6.5 0.0 copy-start.2
  6.5 0.0 all-gather.3.cloned.1.call-start
  6.6 1.7 multiply_reduce_fusion
  8.2 2.8 %convert_element_type.15 = f32[256,2048]{1,0:T(8,128)} convert(bf16[256,2048]{1,0:T(8,128)(2,1)} %param.7) | non-fusion elementwise | flops 524288 | bytes 3145728 | tf_op jit(solution)/shard_map/convert_element_type | solution.py:8
  11.0 0.8 dynamic-slice
  11.8 1.9 fusion.9
  13.6 0.0 all-gather.3.cloned.1.call-update
  13.7 0.0 copy-done.1
  13.7 0.0 copy-done.2
  13.7 0.6 copy.14
  14.3 7.3 %all-to-all-start = ((f32[8,1,256]{2,1,0:T(1,128)}), f32[8,1,256]{2,1,0:T(1,128)S(1)}, u32[]{:S(2)}, u32[]{:S(2)}) async-start(f32[8,1,256]{2,1,0:T(1,128)} %copy.14), calls=%async_computation | async-start | bytes 16384 | tf_op jit(solution)/shard_map/all_to_all | solution.py:72
  21.6 0.0 reduce-scatter.2.cloned.1.call-start
  21.6 4.5 %reshape_squeeze.3 = bf16[512,4,512]{2,1,0:T(4,128)(2,1)} reshape(bf16[1,512,2048]{2,1,0:T(8,128)(2,1)} %param.13) | data formatting | bytes 4194304 | tf_op jit(solution)/shard_map/reshape;squeeze | solution.py:80
  26.1 2.0 all-to-all-done
  28.1 65.5 %all-gather.3.cloned.1.call-done = bf16[8192,512]{1,0:T(8,128)(2,1)} async-done(((bf16[256,512]{1,0:T(8,128)(2,1)}), bf16[8192,512]{1,0:T(8,128)(2,1)}) %all-gather.3.cloned.1.call-update) | async-done | bytes 8388624 | tf_op jit(solution)/shard_map/all_gather | solution.py:73
  93.6 10.4 %fusion.14 = f32[8,256,512,1]{2,1,3,0:T(8,128)} fusion(bf16[8,4,256,512]{3,2,1,0:T(8,128)(2,1)} %bitcast.57, bf16[4,512,512,1]{2,1,0,3:T(8,128)(2,1)} %bitcast.59), kind=kOutput, calls=%fused_computation.24 | convolution fusion | flops 4294967296 | bytes 14680064 | tf_op jit(solution)/shard_map/epcd,pdf->ecf/dot_general | solution.py:78
  104.0 0.0 copy-done
  104.0 15.5 %select_convert_fusion = bf16[8,256,4,512]{3,1,2,0:T(8,128)(2,1)} fusion(f32[8,256]{1,0:T(8,128)S(1)} %bitcast.56, pred[8,256]{1,0:T(8,128)(4,1)S(1)} %broadcast_compare_fusion, bf16[512,4,512]{2,1,0:T(4,128)(2,1)} %reshape_squeeze.3, f32[8,256,512,1]{2,1,3,0:T(8,128)} %fusion.14, bf16[8,4,256,512]{3,2,1,0:T(8,128)(2,1)} %bitcast.58, ...), kind=kOutput, calls=%fused_computation | convolution fusion | flops 8613003264 | bytes 25176064 | tf_op jit(solution)/shard_map/ecf,fpd->epcd/dot_general | solution.py:81
  119.6 0.0 reduce-scatter.2.cloned.1.call-update
  119.6 149.1 %reduce-scatter.2.cloned.1.call-done = bf16[1,256,512]{2,1,0:T(8,128)(2,1)} async-done(((bf16[32,256,512]{2,1,0:T(8,128)(2,1)}), bf16[1,256,512]{2,1,0:T(8,128)(2,1)}) %reduce-scatter.2.cloned.1.call-update) | async-done | bytes 262160 | tf_op jit(solution)/shard_map/reduce_scatter | solution.py:84
  (4 shorter events, 0.0 us)
Async XLA Ops:
  6.5 97.5 %copy-start = (bf16[1,2048,512]{2,1,0:T(8,128)(2,1)S(1)}, bf16[1,2048,512]{2,1,0:T(8,128)(2,1)}, u32[]{:S(2)}) copy-start(bf16[1,2048,512]{2,1,0:T(8,128)(2,1)} %param.11) | copy-start | bytes 6291460
  6.5 7.1 %copy-start.1 = (f32[256,4]{0,1:T(4,128)S(1)}, f32[256,4]{0,1:T(4,128)}, u32[]{:S(2)}) copy-start(f32[256,4]{0,1:T(4,128)} %param.10) | copy-start | bytes 12292
  6.5 7.1 %copy-start.2 = (s32[256,4]{0,1:T(4,128)S(1)}, s32[256,4]{0,1:T(4,128)}, u32[]{:S(2)}) copy-start(s32[256,4]{0,1:T(4,128)} %param.9) | copy-start | bytes 12292
  6.5 87.1 %all-gather.3.cloned.1.call-start = ((), (), s32[]{:S(2)}) async-start(), calls=%async_computation.3 | async-start | bytes 8650752 | tf_op jit(solution)/shard_map/all_gather | solution.py:73
  14.3 13.8 %all-to-all-start = ((f32[8,1,256]{2,1,0:T(1,128)}), f32[8,1,256]{2,1,0:T(1,128)S(1)}, u32[]{:S(2)}, u32[]{:S(2)}) async-start(f32[8,1,256]{2,1,0:T(1,128)} %copy.14), calls=%async_computation | async-start | bytes 16384 | tf_op jit(solution)/shard_map/all_to_all | solution.py:72
  21.6 247.1 %reduce-scatter.2.cloned.1.call-start = ((), (), s32[]{:S(2)}) async-start(), calls=%async_computation.2 | async-start | bytes 8650752 | tf_op jit(solution)/shard_map/reduce_scatter | solution.py:84
Sparse Core Ops, SparseCore 0:
  13.8 79.7 all-gather.2
  119.7 148.9 reduce-scatter.1

commit v2 on v1

--- a/solution.py
+++ b/solution.py
@@ -1,7 +1,14 @@
+import functools
+
 import jax
 import jax.numpy as jnp
 from jax import lax
+from jax.experimental import pallas as pl
+from jax.experimental.pallas import tpu as pltpu
 from jax.sharding import PartitionSpec as P
+
+
+MESH = pl.DeviceIdType.MESH
 
 
 def normalise(tokens, norm_gain):
@@ -59,36 +66,424 @@
     return mixed.astype(jnp.bfloat16)
 
 
+def kernel(
+    n_ep, tokens_ref, gain_ref, route_ref, gate_hbm, up_hbm, down_hbm, out_ref,
+    gath, gate_w, up_w, down_w, hidden, part, dbuf, ya, xa, xb, yb, own, rup, rdn,
+    w_sem, sz, rz, sx, rx, sy, ry, sd, rd,
+    s_d, r_d, s_ya, r_ya, s_xb, r_xb, s_xa, r_xa, s_yb, r_yb, s_z, r_z,
+):
+    ep, tp = lax.axis_index("ep"), lax.axis_index("tp")
+    z, x, y, c = ep // 2, ep % 2, tp // 2, tp % 2
+    nz = n_ep // 2
+    width = tokens_ref.shape[1]
+    quarter = width // 4
+    eighth = quarter // 2
+    common = width // 8
+    special = (width - 2 * common) // 4
+    above = {"ep": lax.rem(ep + 2, n_ep), "tp": tp}
+    below = {"ep": lax.rem(ep + n_ep - 2, n_ep), "tp": tp}
+    xdev = {"ep": 2 * z + 1 - x, "tp": tp}
+    ydev = {"ep": ep, "tp": 2 * (1 - y) + c}
+    ddev = {"ep": ep, "tp": 2 * y + 1 - c}
+
+    weight_copies = [
+        pltpu.make_async_copy(gate_hbm.at[0], gate_w, w_sem.at[0]),
+        pltpu.make_async_copy(up_hbm.at[0], up_w, w_sem.at[1]),
+        pltpu.make_async_copy(down_hbm.at[0], down_w, w_sem.at[2]),
+    ]
+    for item in weight_copies:
+        item.start()
+
+    barrier = pltpu.get_barrier_semaphore()
+
+    def greet(device):
+        pl.semaphore_signal(barrier, inc=1, device_id=device, device_id_type=MESH)
+
+    for device in (xdev, ydev, ddev):
+        greet(device)
+
+    @pl.when(z > 0)
+    def _():
+        greet(below)
+
+    @pl.when(z < nz - 1)
+    def _():
+        greet(above)
+
+    tile = 32
+
+    def norm_step(i, carry):
+        rows = pl.ds(pl.multiple_of(i * tile, tile), tile)
+        values = tokens_ref[rows, :].astype(jnp.float32)
+        scale = lax.rsqrt(jnp.mean(values * values, axis=1, keepdims=True) + 1e-06)
+        gath[ep, rows, :] = (values * scale * gain_ref[...]).astype(jnp.bfloat16)
+        return carry
+
+    lax.fori_loop(0, tokens_ref.shape[0] // tile, norm_step, 0)
+    greeted = 3 + jnp.where(z > 0, 1, 0) + jnp.where(z < nz - 1, 1, 0)
+    pl.semaphore_wait(barrier, greeted)
+
+    def cols(k, yy, cc):
+        if k == 0:
+            return pl.ds(pl.multiple_of(cc * common, 128), common)
+        return pl.ds(pl.multiple_of(2 * common + (2 * yy + cc) * special, 128), special)
+
+    def move(block, k, yy, cc, device, send, recv):
+        ref = gath.at[block, :, cols(k, yy, cc)]
+        return pltpu.make_async_remote_copy(
+            src_ref=ref, dst_ref=ref, send_sem=send, recv_sem=recv,
+            device_id=device, device_id_type=MESH,
+        )
+
+    def go_z(block, k, direction):
+        device = above if direction == 0 else below
+        return move(block, k, y, c, device, sz.at[direction, k, block], rz.at[k, block])
+
+    def go_x(block, k):
+        return move(block, k, y, c, xdev, sx.at[k, block], rx.at[k, block])
+
+    def go_y(block, yy):
+        return move(block, 1, yy, c, ydev, sy.at[block], ry.at[block])
+
+    def go_d(block, kind, cc):
+        k, yy = (0, y) if kind == 0 else (1, y if kind == 1 else 1 - y)
+        return move(block, k, yy, cc, ddev, sd.at[kind, block], rd.at[kind, block])
+
+    for k in (0, 1):
+        @pl.when(z < nz - 1)
+        def _():
+            go_z(ep, k, 0).start()
+
+        @pl.when(z > 0)
+        def _():
+            go_z(ep, k, 1).start()
+
+        go_x(ep, k).start()
+
+    def from_z(block, direction):
+        for k in (1, 0):
+            go_z(block, k, direction).wait_recv()
+
+            @pl.when(z < nz - 1 if direction == 0 else z > 0)
+            def _():
+                go_z(block, k, direction).start()
+
+            go_x(block, k).start()
+            if k == 1:
+                go_y(block, y).start()
+            go_d(block, k, c).start()
+
+    def from_x(block):
+        for k in (1, 0):
+            go_x(block, k).wait_recv()
+            if k == 1:
+                go_y(block, y).start()
+            go_d(block, k, c).start()
+
+    def from_y(block):
+        go_y(block, 1 - y).wait_recv()
+        go_d(block, 2, c).start()
+
+    def at_distance(s, action):
+        @pl.when(z - s >= 0)
+        def _():
+            action(z - s, 0)
+
+        @pl.when(z + s <= nz - 1)
+        def _():
+            action(z + s, 1)
+
+    for s in range(1, nz):
+        at_distance(s, lambda row, way: from_z(2 * row + x, way))
+        if s == 1:
+            from_x(2 * z + 1 - x)
+        else:
+            at_distance(s - 1, lambda row, way: from_x(2 * row + 1 - x))
+    at_distance(nz - 1, lambda row, way: from_x(2 * row + 1 - x))
+
+    from_y(2 * z + 1 - x)
+    for s in range(1, nz):
+        at_distance(s, lambda row, way: from_y(2 * row + x))
+        at_distance(s, lambda row, way: from_y(2 * row + 1 - x))
+
+    def others(action):
+        action(2 * z + 1 - x)
+        for s in range(1, nz):
+            at_distance(s, lambda row, way: action(2 * row + x))
+            at_distance(s, lambda row, way: action(2 * row + 1 - x))
+
+    def arrived(block):
+        for kind in (0, 1, 2):
+            go_d(block, kind, 1 - c).wait_recv()
+
+    others(arrived)
+    for item in weight_copies:
+        item.wait()
+
+    def span(start, size):
+        return pl.ds(pl.multiple_of(start, 128), size)
+
+    def send(src, dst, send_sem, recv_sem, device):
+        return pltpu.make_async_remote_copy(
+            src_ref=src, dst_ref=dst, send_sem=send_sem, recv_sem=recv_sem,
+            device_id=device, device_id_type=MESH,
+        )
+
+    def d_copy(r, yq, cc):
+        return send(
+            part.at[pl.ds(2 * r, 2), :, span((2 * yq + cc) * quarter, quarter)],
+            dbuf.at[pl.ds(2 * r, 2), :, span(yq * quarter, quarter)],
+            s_d.at[r, yq], r_d.at[r, yq], ddev,
+        )
+
+    def ya_copy(r):
+        return send(
+            dbuf.at[pl.ds(2 * r, 2), :, span((1 - y) * quarter, eighth)],
+            ya.at[pl.ds(2 * r, 2)], s_ya.at[r], r_ya.at[r], ydev,
+        )
+
+    def xb_copy(r, yq):
+        return send(
+            dbuf.at[2 * r + 1 - x, :, span(yq * quarter + eighth, eighth)],
+            xb.at[r, :, span(yq * eighth, eighth)], s_xb.at[r, yq], r_xb.at[r, yq], xdev,
+        )
+
+    def xa_copy(r):
+        return send(ya.at[2 * r + 1 - x], xa.at[r], s_xa.at[r], r_xa.at[r], xdev)
+
+    def yb_copy(r):
+        return send(
+            xb.at[r, :, span((1 - y) * eighth, eighth)],
+            yb.at[r], s_yb.at[r], r_yb.at[r], ydev,
+        )
+
+    def up_copy(r):
+        return send(own.at[r], rup.at[r], s_z.at[0, r], r_z.at[0, r], above)
+
+    def dn_copy(r):
+        return send(own.at[r], rdn.at[r], s_z.at[1, r], r_z.at[1, r], below)
+
+    def add(a, b):
+        return (a.astype(jnp.float32) + b.astype(jnp.float32)).astype(jnp.bfloat16)
+
+    rows = tokens_ref.shape[0]
+    ff = gate_w.shape[1]
+    fstep = min(256, ff)
+
+    def compute(r):
+        lhs_of = lambda: gath[pl.ds(2 * r, 2)].reshape(2 * rows, width)
+        route = route_ref[pl.ds(2 * r, 2)].reshape(2 * rows, 128)
+        route = jnp.concatenate([route] * (fstep // 128), axis=1)
+
+        def ff_step(j, carry):
+            at = span(j * fstep, fstep)
+            lhs = lhs_of()
+            gate = jnp.dot(lhs, gate_w[:, at], preferred_element_type=jnp.float32)
+            upper = jnp.dot(lhs, up_w[:, at], preferred_element_type=jnp.float32)
+            value = activate(gate, upper)
+            hidden[:, at] = jnp.where(route > 0, route * value, 0.0).astype(jnp.bfloat16)
+            return carry
+
+        lax.fori_loop(0, ff // fstep, ff_step, 0)
+
+        def down_step(j, carry):
+            yq = j % 2
+            cc = jnp.where(j < 2, 1 - c, c)
+            at = span((2 * yq + cc) * quarter, quarter)
+            value = jnp.dot(hidden[...], down_w[:, at], preferred_element_type=jnp.float32)
+            part[pl.ds(2 * r, 2), :, at] = value.astype(jnp.bfloat16).reshape(2, rows, quarter)
+
+            @pl.when(j < 2)
+            def _():
+                d_copy(r, yq, 1 - c).start()
+
+            return carry
+
+        lax.fori_loop(0, 4, down_step, 0)
+
+    def stage_a(r):
+        for yq in (0, 1):
+            d_copy(r, yq, 1 - c).wait_recv()
+            mine = part[pl.ds(2 * r, 2), :, span((2 * yq + c) * quarter, quarter)]
+            at = span(yq * quarter, quarter)
+            dbuf[pl.ds(2 * r, 2), :, at] = add(mine, dbuf[pl.ds(2 * r, 2), :, at])
+        ya_copy(r).start()
+        for yq in (0, 1):
+            xb_copy(r, yq).start()
+
+    def stage_b(r):
+        ya_copy(r).wait_recv()
+        ya[pl.ds(2 * r, 2)] = add(
+            dbuf[pl.ds(2 * r, 2), :, span(y * quarter, eighth)], ya[pl.ds(2 * r, 2)]
+        )
+        xa_copy(r).start()
+        for yq in (0, 1):
+            xb_copy(r, yq).wait_recv()
+            at = span(yq * eighth, eighth)
+            mine = dbuf[2 * r + x, :, span(yq * quarter + eighth, eighth)]
+            xb[r, :, at] = add(mine, xb[r, :, at])
+        yb_copy(r).start()
+
+    def stage_c(r):
+        xa_copy(r).wait_recv()
+        own[r, :, 0:eighth] = add(ya[2 * r + x], xa[r])
+        yb_copy(r).wait_recv()
+        own[r, :, eighth:quarter] = add(xb[r, :, span(y * eighth, eighth)], yb[r])
+
+    def stage_d(r):
+        @pl.when((z > 0) & (z <= r))
+        def _():
+            up_copy(r).wait_recv()
+            own[r] = add(own[r], rup[r])
+
+        @pl.when((z < nz - 1) & (z >= r))
+        def _():
+            dn_copy(r).wait_recv()
+            own[r] = add(own[r], rdn[r])
+
+        @pl.when(z < r)
+        def _():
+            up_copy(r).start()
+
+        @pl.when(z > r)
+        def _():
+            dn_copy(r).start()
+
+        @pl.when(z == r)
+        def _():
+            out_ref[...] = own[r]
+
+    def row_of(i):
+        odd = i % 2
+        return (1 - odd) * (nz - 1 - i // 2) + odd * (i // 2)
+
+    def step(i, carry):
+        @pl.when(i < nz)
+        def _():
+            compute(row_of(i))
+            stage_a(row_of(i))
+
+        @pl.when((i >= 1) & (i < nz + 1))
+        def _():
+            stage_b(row_of(i - 1))
+
+        @pl.when((i >= 2) & (i < nz + 2))
+        def _():
+            stage_c(row_of(i - 2))
+            stage_d(row_of(i - 2))
+
+        return carry
+
+    lax.fori_loop(0, nz + 2, step, 0)
+
+    def sent(block, direction):
+        for k in (0, 1):
+            @pl.when(z < nz - 1 if direction == 0 else z > 0)
+            def _():
+                go_z(block, k, direction).wait_send()
+
+            go_x(block, k).wait_send()
+
+    for k in (0, 1):
+        @pl.when(z < nz - 1)
+        def _():
+            go_z(ep, k, 0).wait_send()
+
+        @pl.when(z > 0)
+        def _():
+            go_z(ep, k, 1).wait_send()
+
+        go_x(ep, k).wait_send()
+    for s in range(1, nz):
+        at_distance(s, lambda row, way: sent(2 * row + x, way))
+
+    def passed(block):
+        go_y(block, y).wait_send()
+        for kind in (0, 1, 2):
+            go_d(block, kind, c).wait_send()
+
+    others(passed)
+
+    def finish(r, carry):
+        for yq in (0, 1):
+            d_copy(r, yq, 1 - c).wait_send()
+            xb_copy(r, yq).wait_send()
+        ya_copy(r).wait_send()
+        xa_copy(r).wait_send()
+        yb_copy(r).wait_send()
+
+        @pl.when(z < r)
+        def _():
+            up_copy(r).wait_send()
+
+        @pl.when(z > r)
+        def _():
+            dn_copy(r).wait_send()
+
+        return carry
+
+    lax.fori_loop(0, nz, finish, 0)
+
+
 def dense(tokens, norm_gain, expert_ids, route_weights, gate_weight, up_weight, down_weight):
-    tok_dev, width = tokens.shape
+    rows, width = tokens.shape
     n_ep = lax.axis_size("ep")
-    n_tp = lax.axis_size("tp")
-    quarter = width // n_tp
-    mine = lax.axis_index("ep")
-    normed = normalise(tokens, norm_gain)
-    columns = lax.dynamic_slice_in_dim(normed, lax.axis_index("tp") * quarter, quarter, 1)
+    nz = n_ep // 2
+    ff = gate_weight.shape[2]
+    quarter = width // lax.axis_size("tp")
+    eighth = quarter // 2
     onehot = expert_ids[:, :, None] == jnp.arange(n_ep, dtype=jnp.int32)[None, None, :]
     table = jnp.sum(jnp.where(onehot, route_weights[:, :, None], 0.0), axis=1)
     weights = lax.all_to_all(table.T, "ep", split_axis=0, concat_axis=0, tiled=True)
-    every = lax.all_gather(columns, ("ep", "tp"), axis=0, tiled=False)
-    every = every.reshape(n_ep, n_tp, tok_dev, quarter)
-    gate_w = gate_weight.reshape(n_tp, quarter, -1)
-    up_w = up_weight.reshape(n_tp, quarter, -1)
-    gate = jnp.einsum("epcd,pdf->ecf", every, gate_w, preferred_element_type=jnp.float32)
-    upper = jnp.einsum("epcd,pdf->ecf", every, up_w, preferred_element_type=jnp.float32)
-    hidden = activate(gate, upper).astype(jnp.bfloat16)
-    down_w = down_weight[0].reshape(-1, n_tp, quarter)
-    out = jnp.einsum("ecf,fpd->epcd", hidden, down_w, preferred_element_type=jnp.float32)
-    out = jnp.where(weights[:, None, :, None] > 0, weights[:, None, :, None] * out, 0.0)
-    out = out.astype(jnp.bfloat16).reshape(n_ep * n_tp, tok_dev, quarter)
-    return lax.psum_scatter(out, ("ep", "tp"), scatter_dimension=0, tiled=False)
+    weights = jnp.broadcast_to(weights[:, :, None], (n_ep, rows, 128))
+    vmem = pl.BlockSpec(memory_space=pltpu.VMEM)
+    hbm = pl.BlockSpec(memory_space=pl.ANY)
+    bf16 = jnp.bfloat16
+    dma = pltpu.SemaphoreType.DMA
+    return pl.pallas_call(
+        functools.partial(kernel, n_ep),
+        out_shape=jax.ShapeDtypeStruct((rows, quarter), bf16),
+        in_specs=[vmem, vmem, vmem, hbm, hbm, hbm],
+        out_specs=vmem,
+        scratch_shapes=[
+            pltpu.VMEM((n_ep, rows, width), bf16),
+            pltpu.VMEM((width, ff), bf16),
+            pltpu.VMEM((width, ff), bf16),
+            pltpu.VMEM((ff, width), bf16),
+            pltpu.VMEM((2 * rows, ff), bf16),
+            pltpu.VMEM((n_ep, rows, width), bf16),
+            pltpu.VMEM((n_ep, rows, 2 * quarter), bf16),
+            pltpu.VMEM((n_ep, rows, eighth), bf16),
+            pltpu.VMEM((nz, rows, eighth), bf16),
+            pltpu.VMEM((nz, rows, 2 * eighth), bf16),
+            pltpu.VMEM((nz, rows, eighth), bf16),
+            pltpu.VMEM((nz, rows, quarter), bf16),
+            pltpu.VMEM((nz, rows, quarter), bf16),
+            pltpu.VMEM((nz, rows, quarter), bf16),
+            dma((3,)),
+            dma((2, 2, n_ep)), dma((2, n_ep)),
+            dma((2, n_ep)), dma((2, n_ep)),
+            dma((n_ep,)), dma((n_ep,)),
+            dma((3, n_ep)), dma((3, n_ep)),
+            dma((nz, 2)), dma((nz, 2)),
+            dma((nz,)), dma((nz,)),
+            dma((nz, 2)), dma((nz, 2)),
+            dma((nz,)), dma((nz,)),
+            dma((nz,)), dma((nz,)),
+            dma((2, nz)), dma((2, nz)),
+        ],
+        compiler_params=pltpu.CompilerParams(
+            collective_id=0, has_side_effects=True, vmem_limit_bytes=60 * 1024 * 1024
+        ),
+    )(tokens, norm_gain[None, :], weights, gate_weight, up_weight, down_weight)
 
 
 def per_device(tokens, norm_gain, expert_ids, route_weights, gate_weight, up_weight, down_weight):
     tok_dev, top = expert_ids.shape
     experts = gate_weight.shape[0] * lax.axis_size("ep")
     whole = gate_weight.shape[0] == 1 and 2 * tok_dev * top // experts >= tok_dev
-    form = dense if whole else routed
+    whole = whole and lax.axis_size("tp") == 4 and lax.axis_size("ep") % 2 == 0
+    form = dense if whole and tokens.shape[1] % 2048 == 0 else routed
     return form(
         tokens, norm_gain, expert_ids, route_weights, gate_weight, up_weight, down_weight
     )

time: 276 us -> 152 us (0.55)
  the two profiles are of different devices: /device:TPU:0 before, /device:TPU:8 now
where the time goes in v2:
time: 152 us
  Pallas kernels  137 us (90%)
  blocking collectives  11.1 us (7%)
  local copies, waits for them, and re-layouts  3.01 us (2%)
    pallas_call x1, Pallas kernels, dense(): pl.pallas_call(functools.partial(kernel, n_ep), out_shape=jax.ShapeDtypeS...  137 us
    all_to_all x1, blocking collectives, dense(): lax.all_to_all(table.T, 'ep', split_axis=0, concat_axis=0, tiled=True)  11.1 us

profile of v2, /device:TPU:8, one launch (start us, length us, event | category | flops | bytes accessed | tf_op | source)
XLA Modules:
  0.0 151.9 jit_solution(7342399776220531705)
XLA Ops:
  0.0 0.7 select_reduce_fusion
  0.7 11.1 %all_to_all.9 = f32[8,1,256]{2,1,0:T(1,128)S(1)} all-to-all(f32[8,1,256]{2,1,0:T(1,128)S(1)} %copy.12), channel_id=1, replica_groups=mesh['ep'=8,'tp'=4] {'ep'}, dimensions={0} | all-to-all | bytes 16384 | tf_op jit(solution)/shard_map/all_to_all | solution.py:437
  11.8 1.3 broadcast_in_dim.30.route_ref
  13.1 137.1 %shard_map.73 = bf16[256,512]{1,0:T(8,128)(2,1)} custom-call(bf16[256,2048]{1,0:T(8,128)(2,1)} %tokens_ref.1, f32[1,2048]{1,0:T(1,128)} %bitcast.9, f32[8,256,128]{2,1,0:T(8,128)} %broadcast_in_dim.30.route_ref, bf16[1,2048,512]{2,1,0:T(8,128)(2,1)} %gate_hbm.1, bf16[1,2048,512]{2,1,0:T(8,128)(2,1)} %up_hbm.1, bf16[1,512,2048]{2,1,0:T(8,128)(2,1)} %down_hbm.1), custom_call_target="tpu_custom_call" | custom-call | tf_op jit(solution)/shard_map/pallas_call | solution.py:443
  150.2 1.7 %copy.17 = bf16[256,512]{1,0:T(8,128)(2,1)} copy(bf16[256,512]{1,0:T(8,128)(2,1)} %shard_map.73) | data formatting | bytes 524288
  (2 shorter events, 0.0 us)

commit v3 on v2

--- a/solution.py
+++ b/solution.py
@@ -68,7 +68,7 @@
 
 def kernel(
     n_ep, tokens_ref, gain_ref, route_ref, gate_hbm, up_hbm, down_hbm, out_ref,
-    gath, gate_w, up_w, down_w, hidden, part, dbuf, ya, xa, xb, yb, own, rup, rdn,
+    gath, gtab, route_buf, gate_w, up_w, down_w, hidden, part, dbuf, ya, xa, xb, yb, own, rup, rdn,
     w_sem, sz, rz, sx, rx, sy, ry, sd, rd,
     s_d, r_d, s_ya, r_ya, s_xb, r_xb, s_xa, r_xa, s_yb, r_yb, s_z, r_z,
 ):
@@ -120,6 +120,7 @@
         return carry
 
     lax.fori_loop(0, tokens_ref.shape[0] // tile, norm_step, 0)
+    gtab[ep] = route_ref[...]
     greeted = 3 + jnp.where(z > 0, 1, 0) + jnp.where(z < nz - 1, 1, 0)
     pl.semaphore_wait(barrier, greeted)
 
@@ -129,7 +130,7 @@
         return pl.ds(pl.multiple_of(2 * common + (2 * yy + cc) * special, 128), special)
 
     def move(block, k, yy, cc, device, send, recv):
-        ref = gath.at[block, :, cols(k, yy, cc)]
+        ref = gtab.at[block] if k == 2 else gath.at[block, :, cols(k, yy, cc)]
         return pltpu.make_async_remote_copy(
             src_ref=ref, dst_ref=ref, send_sem=send, recv_sem=recv,
             device_id=device, device_id_type=MESH,
@@ -149,7 +150,7 @@
         k, yy = (0, y) if kind == 0 else (1, y if kind == 1 else 1 - y)
         return move(block, k, yy, cc, ddev, sd.at[kind, block], rd.at[kind, block])
 
-    for k in (0, 1):
+    for k in (1, 2, 0):
         @pl.when(z < nz - 1)
         def _():
             go_z(ep, k, 0).start()
@@ -161,7 +162,7 @@
         go_x(ep, k).start()
 
     def from_z(block, direction):
-        for k in (1, 0):
+        for k in (1, 2, 0):
             go_z(block, k, direction).wait_recv()
 
             @pl.when(z < nz - 1 if direction == 0 else z > 0)
@@ -171,14 +172,16 @@
             go_x(block, k).start()
             if k == 1:
                 go_y(block, y).start()
-            go_d(block, k, c).start()
+            if k < 2:
+                go_d(block, k, c).start()
 
     def from_x(block):
-        for k in (1, 0):
+        for k in (1, 2, 0):
             go_x(block, k).wait_recv()
             if k == 1:
                 go_y(block, y).start()
-            go_d(block, k, c).start()
+            if k < 2:
+                go_d(block, k, c).start()
 
     def from_y(block):
         go_y(block, 1 - y).wait_recv()
@@ -201,11 +204,6 @@
             at_distance(s - 1, lambda row, way: from_x(2 * row + 1 - x))
     at_distance(nz - 1, lambda row, way: from_x(2 * row + 1 - x))
 
-    from_y(2 * z + 1 - x)
-    for s in range(1, nz):
-        at_distance(s, lambda row, way: from_y(2 * row + x))
-        at_distance(s, lambda row, way: from_y(2 * row + 1 - x))
-
     def others(action):
         action(2 * z + 1 - x)
         for s in range(1, nz):
@@ -216,10 +214,6 @@
         for kind in (0, 1, 2):
             go_d(block, kind, 1 - c).wait_recv()
 
-    others(arrived)
-    for item in weight_copies:
-        item.wait()
-
     def span(start, size):
         return pl.ds(pl.multiple_of(start, 128), size)
 
@@ -272,8 +266,12 @@
 
     def compute(r):
         lhs_of = lambda: gath[pl.ds(2 * r, 2)].reshape(2 * rows, width)
-        route = route_ref[pl.ds(2 * r, 2)].reshape(2 * rows, 128)
-        route = jnp.concatenate([route] * (fstep // 128), axis=1)
+        for j in (0, 1):
+            flipped = jnp.transpose(gtab[2 * r + j])
+            lane = lax.broadcasted_iota(jnp.int32, flipped.shape, 1)
+            column = jnp.sum(jnp.where(lane == ep, flipped, 0.0), axis=1, keepdims=True)
+            route_buf[j * rows:(j + 1) * rows, :] = jnp.broadcast_to(column, (rows, 128))
+        route = jnp.concatenate([route_buf[...]] * (fstep // 128), axis=1)
 
         def ff_step(j, carry):
             at = span(j * fstep, fstep)
@@ -353,11 +351,36 @@
         def _():
             out_ref[...] = own[r]
 
+    last_first = [nz - 1 - i // 2 if i % 2 == 0 else i // 2 for i in range(nz)]
+    order = [[k] + [r for r in last_first if r != k] for k in range(nz)]
+    due = [[order[k].index(r) + 2 for r in range(nz)] for k in range(nz)]
+    for r in range(nz):
+        for k in range(1, r):
+            due[k][r] = max(due[k][r], due[k - 1][r] + 1)
+        for k in range(nz - 2, r, -1):
+            due[k][r] = max(due[k][r], due[k + 1][r] + 1)
+        for k in (r - 1, r + 1):
+            if 0 <= k < nz:
+                due[r][r] = max(due[r][r], due[k][r] + 1)
+    steps = max(max(line) for line in due) + 1
+
     def row_of(i):
-        odd = i % 2
-        return (1 - odd) * (nz - 1 - i // 2) + odd * (i // 2)
+        row = z
+        for k in range(nz):
+            for j in range(1, nz):
+                row = jnp.where((z == k) & (i == j), order[k][j], row)
+        return row
 
     def step(i, carry):
+        @pl.when(i == 1)
+        def _():
+            for s in range(1, nz):
+                at_distance(s, lambda row, way: from_y(2 * row + x))
+                at_distance(s, lambda row, way: from_y(2 * row + 1 - x))
+            for s in range(1, nz):
+                at_distance(s, lambda row, way: arrived(2 * row + x))
+                at_distance(s, lambda row, way: arrived(2 * row + 1 - x))
+
         @pl.when(i < nz)
         def _():
             compute(row_of(i))
@@ -370,21 +393,37 @@
         @pl.when((i >= 2) & (i < nz + 2))
         def _():
             stage_c(row_of(i - 2))
-            stage_d(row_of(i - 2))
-
+
+        def chain(r, inner):
+            when = 0
+            for k in range(nz):
+                for j in range(nz):
+                    when = jnp.where((z == k) & (r == j), due[k][j], when)
+
+            @pl.when(i == when)
+            def _():
+                stage_d(r)
+
+            return inner
+
+        lax.fori_loop(0, nz, chain, 0)
         return carry
 
-    lax.fori_loop(0, nz + 2, step, 0)
+    from_y(2 * z + 1 - x)
+    arrived(2 * z + 1 - x)
+    for item in weight_copies:
+        item.wait()
+    lax.fori_loop(0, steps, step, 0)
 
     def sent(block, direction):
-        for k in (0, 1):
+        for k in (0, 1, 2):
             @pl.when(z < nz - 1 if direction == 0 else z > 0)
             def _():
                 go_z(block, k, direction).wait_send()
 
             go_x(block, k).wait_send()
 
-    for k in (0, 1):
+    for k in (0, 1, 2):
         @pl.when(z < nz - 1)
         def _():
             go_z(ep, k, 0).wait_send()
@@ -434,8 +473,6 @@
     eighth = quarter // 2
     onehot = expert_ids[:, :, None] == jnp.arange(n_ep, dtype=jnp.int32)[None, None, :]
     table = jnp.sum(jnp.where(onehot, route_weights[:, :, None], 0.0), axis=1)
-    weights = lax.all_to_all(table.T, "ep", split_axis=0, concat_axis=0, tiled=True)
-    weights = jnp.broadcast_to(weights[:, :, None], (n_ep, rows, 128))
     vmem = pl.BlockSpec(memory_space=pltpu.VMEM)
     hbm = pl.BlockSpec(memory_space=pl.ANY)
     bf16 = jnp.bfloat16
@@ -447,6 +484,8 @@
         out_specs=vmem,
         scratch_shapes=[
             pltpu.VMEM((n_ep, rows, width), bf16),
+            pltpu.VMEM((n_ep, n_ep, rows), jnp.float32),
+            pltpu.VMEM((2 * rows, 128), jnp.float32),
             pltpu.VMEM((width, ff), bf16),
             pltpu.VMEM((width, ff), bf16),
             pltpu.VMEM((ff, width), bf16),
@@ -461,8 +500,8 @@
             pltpu.VMEM((nz, rows, quarter), bf16),
             pltpu.VMEM((nz, rows, quarter), bf16),
             dma((3,)),
-            dma((2, 2, n_ep)), dma((2, n_ep)),
-            dma((2, n_ep)), dma((2, n_ep)),
+            dma((2, 3, n_ep)), dma((3, n_ep)),
+            dma((3, n_ep)), dma((3, n_ep)),
             dma((n_ep,)), dma((n_ep,)),
             dma((3, n_ep)), dma((3, n_ep)),
             dma((nz, 2)), dma((nz, 2)),
@@ -475,7 +514,7 @@
         compiler_params=pltpu.CompilerParams(
             collective_id=0, has_side_effects=True, vmem_limit_bytes=60 * 1024 * 1024
         ),
-    )(tokens, norm_gain[None, :], weights, gate_weight, up_weight, down_weight)
+    )(tokens, norm_gain[None, :], table.T, gate_weight, up_weight, down_weight)
 
 
 def per_device(tokens, norm_gain, expert_ids, route_weights, gate_weight, up_weight, down_weight):

time: 152 us -> 105 us (0.69)
  Pallas kernels: 137 us -> 102 us
  blocking collectives: 11.1 us -> 0 us
    pallas_call x1, Pallas kernels: 137 us -> 102 us  [dense(): pl.pallas_call(functools.partial(kernel, n_ep), out_shape=jax.ShapeDtypeS...]
    all_to_all x1 -> x0, blocking collectives: 11.1 us -> none  [dense(): lax.all_to_all(table.T, 'ep', split_axis=0, concat_axis=0, tiled=True)]
where the time goes in v3:
time: 105 us
  Pallas kernels  102 us (97%)
  local copies, waits for them, and re-layouts  1.67 us (2%)
  other arithmetic  1.31 us (1%)
    pallas_call x1, Pallas kernels, dense(): pl.pallas_call(functools.partial(kernel, n_ep), out_shape=jax.ShapeDtypeS...  102 us

profile of v3, /device:TPU:8, one launch (start us, length us, event | category | flops | bytes accessed | tf_op | source)
XLA Modules:
  0.0 105.2 jit_solution(1873351140423632664)
XLA Ops:
  0.0 1.3 %select_reduce_fusion = f32[256,8]{0,1:T(8,128)} fusion(f32[256,4]{0,1:T(4,128)} %param.10, s32[256,4]{0,1:T(4,128)} %param.9), kind=kLoop, calls=%fused_computation | loop fusion | flops 22528 | bytes 16384 | tf_op jit(solution)/shard_map/reduce_sum | solution.py:475
  1.3 102.2 %shard_map.73 = bf16[256,512]{1,0:T(8,128)(2,1)} custom-call(bf16[256,2048]{1,0:T(8,128)(2,1)} %tokens_ref.1, f32[1,2048]{1,0:T(1,128)} %bitcast.3, f32[8,256]{1,0:T(8,128)} %bitcast.2, bf16[1,2048,512]{2,1,0:T(8,128)(2,1)} %gate_hbm.1, bf16[1,2048,512]{2,1,0:T(8,128)(2,1)} %up_hbm.1, bf16[1,512,2048]{2,1,0:T(8,128)(2,1)} %down_hbm.1), custom_call_target="tpu_custom_call" | custom-call | tf_op jit(solution)/shard_map/pallas_call | solution.py:480
  103.5 1.7 %copy.11 = bf16[256,512]{1,0:T(8,128)(2,1)} copy(bf16[256,512]{1,0:T(8,128)(2,1)} %shard_map.73) | data formatting | bytes 524288

commit v4 on v3

--- a/solution.py
+++ b/solution.py
@@ -68,7 +68,7 @@
 
 def kernel(
     n_ep, tokens_ref, gain_ref, route_ref, gate_hbm, up_hbm, down_hbm, out_ref,
-    gath, gtab, route_buf, gate_w, up_w, down_w, hidden, part, dbuf, ya, xa, xb, yb, own, rup, rdn,
+    gath, gtab, route_buf, gate_w, up_w, down_w, hidden, part, dbuf, ya, xa, xb, yb, own, zin,
     w_sem, sz, rz, sx, rx, sy, ry, sd, rd,
     s_d, r_d, s_ya, r_ya, s_xb, r_xb, s_xa, r_xa, s_yb, r_yb, s_z, r_z,
 ):
@@ -102,13 +102,11 @@
     for device in (xdev, ydev, ddev):
         greet(device)
 
-    @pl.when(z > 0)
-    def _():
-        greet(below)
-
-    @pl.when(z < nz - 1)
-    def _():
-        greet(above)
+    def peer(k):
+        return {"ep": lax.rem(ep + 2 * k, n_ep), "tp": tp}
+
+    for k in range(1, nz):
+        greet(peer(k))
 
     tile = 32
 
@@ -121,8 +119,7 @@
 
     lax.fori_loop(0, tokens_ref.shape[0] // tile, norm_step, 0)
     gtab[ep] = route_ref[...]
-    greeted = 3 + jnp.where(z > 0, 1, 0) + jnp.where(z < nz - 1, 1, 0)
-    pl.semaphore_wait(barrier, greeted)
+    pl.semaphore_wait(barrier, 2 + nz)
 
     def cols(k, yy, cc):
         if k == 0:
@@ -223,51 +220,75 @@
             device_id=device, device_id_type=MESH,
         )
 
-    def d_copy(r, yq, cc):
-        return send(
-            part.at[pl.ds(2 * r, 2), :, span((2 * yq + cc) * quarter, quarter)],
-            dbuf.at[pl.ds(2 * r, 2), :, span(yq * quarter, quarter)],
-            s_d.at[r, yq], r_d.at[r, yq], ddev,
-        )
-
-    def ya_copy(r):
-        return send(
-            dbuf.at[pl.ds(2 * r, 2), :, span((1 - y) * quarter, eighth)],
-            ya.at[pl.ds(2 * r, 2)], s_ya.at[r], r_ya.at[r], ydev,
-        )
-
-    def xb_copy(r, yq):
-        return send(
-            dbuf.at[2 * r + 1 - x, :, span(yq * quarter + eighth, eighth)],
-            xb.at[r, :, span(yq * eighth, eighth)], s_xb.at[r, yq], r_xb.at[r, yq], xdev,
-        )
-
-    def xa_copy(r):
-        return send(ya.at[2 * r + 1 - x], xa.at[r], s_xa.at[r], r_xa.at[r], xdev)
-
-    def yb_copy(r):
-        return send(
-            xb.at[r, :, span((1 - y) * eighth, eighth)],
-            yb.at[r], s_yb.at[r], r_yb.at[r], ydev,
-        )
-
-    def up_copy(r):
-        return send(own.at[r], rup.at[r], s_z.at[0, r], r_z.at[0, r], above)
-
-    def dn_copy(r):
-        return send(own.at[r], rdn.at[r], s_z.at[1, r], r_z.at[1, r], below)
+    pieces = 2
+    rows = tokens_ref.shape[0] // pieces
+
+    def half(u):
+        return pl.ds(pl.multiple_of((u % pieces) * rows, 16), rows)
+
+    def half_lane(u):
+        return pl.ds(pl.multiple_of((u % pieces) * rows, 128), rows)
+
+    def d_copy(u, yq, cc):
+        r = u // pieces
+        return send(
+            part.at[pl.ds(2 * r, 2), half(u), span((2 * yq + cc) * quarter, quarter)],
+            dbuf.at[pl.ds(2 * r, 2), half(u), span(yq * quarter, quarter)],
+            s_d.at[u, yq], r_d.at[u, yq], ddev,
+        )
+
+    def ya_copy(u):
+        r = u // pieces
+        return send(
+            dbuf.at[pl.ds(2 * r, 2), half(u), span((1 - y) * quarter, eighth)],
+            ya.at[pl.ds(2 * r, 2), half(u)], s_ya.at[u], r_ya.at[u], ydev,
+        )
+
+    def xb_copy(u, yq):
+        r = u // pieces
+        return send(
+            dbuf.at[2 * r + 1 - x, half(u), span(yq * quarter + eighth, eighth)],
+            xb.at[r, half(u), span(yq * eighth, eighth)],
+            s_xb.at[u, yq], r_xb.at[u, yq], xdev,
+        )
+
+    def xa_copy(u):
+        r = u // pieces
+        return send(
+            ya.at[2 * r + 1 - x, half(u)], xa.at[r, half(u)], s_xa.at[u], r_xa.at[u], xdev
+        )
+
+    def yb_copy(u):
+        r = u // pieces
+        return send(
+            xb.at[r, half(u), span((1 - y) * eighth, eighth)],
+            yb.at[r, half(u)], s_yb.at[u], r_yb.at[u], ydev,
+        )
+
+    def z_copy(u, row):
+        p = u % pieces
+        return send(
+            own.at[row, half(u)], zin.at[z, half(u)], s_z.at[u], r_z.at[z, p],
+            {"ep": 2 * row + x, "tp": tp},
+        )
+
+    def z_wait(origin, p):
+        return send(
+            own.at[origin, half(p)], zin.at[origin, half(p)], s_z.at[p], r_z.at[origin, p],
+            {"ep": 2 * origin + x, "tp": tp},
+        )
 
     def add(a, b):
         return (a.astype(jnp.float32) + b.astype(jnp.float32)).astype(jnp.bfloat16)
 
-    rows = tokens_ref.shape[0]
     ff = gate_w.shape[1]
     fstep = min(256, ff)
 
-    def compute(r):
-        lhs_of = lambda: gath[pl.ds(2 * r, 2)].reshape(2 * rows, width)
+    def compute(u):
+        r = u // pieces
+        lhs_of = lambda: gath[pl.ds(2 * r, 2), half(u)].reshape(2 * rows, width)
         for j in (0, 1):
-            flipped = jnp.transpose(gtab[2 * r + j])
+            flipped = jnp.transpose(gtab[2 * r + j, :, half_lane(u)])
             lane = lax.broadcasted_iota(jnp.int32, flipped.shape, 1)
             column = jnp.sum(jnp.where(lane == ep, flipped, 0.0), axis=1, keepdims=True)
             route_buf[j * rows:(j + 1) * rows, :] = jnp.broadcast_to(column, (rows, 128))
@@ -289,90 +310,71 @@
             cc = jnp.where(j < 2, 1 - c, c)
             at = span((2 * yq + cc) * quarter, quarter)
             value = jnp.dot(hidden[...], down_w[:, at], preferred_element_type=jnp.float32)
-            part[pl.ds(2 * r, 2), :, at] = value.astype(jnp.bfloat16).reshape(2, rows, quarter)
+            part[pl.ds(2 * r, 2), half(u), at] = value.astype(jnp.bfloat16).reshape(2, rows, quarter)
 
             @pl.when(j < 2)
             def _():
-                d_copy(r, yq, 1 - c).start()
+                d_copy(u, yq, 1 - c).start()
 
             return carry
 
         lax.fori_loop(0, 4, down_step, 0)
 
-    def stage_a(r):
+    def stage_a(u):
+        r = u // pieces
         for yq in (0, 1):
-            d_copy(r, yq, 1 - c).wait_recv()
-            mine = part[pl.ds(2 * r, 2), :, span((2 * yq + c) * quarter, quarter)]
+            d_copy(u, yq, 1 - c).wait_recv()
+            mine = part[pl.ds(2 * r, 2), half(u), span((2 * yq + c) * quarter, quarter)]
             at = span(yq * quarter, quarter)
-            dbuf[pl.ds(2 * r, 2), :, at] = add(mine, dbuf[pl.ds(2 * r, 2), :, at])
-        ya_copy(r).start()
+            dbuf[pl.ds(2 * r, 2), half(u), at] = add(mine, dbuf[pl.ds(2 * r, 2), half(u), at])
+        ya_copy(u).start()
         for yq in (0, 1):
-            xb_copy(r, yq).start()
-
-    def stage_b(r):
-        ya_copy(r).wait_recv()
-        ya[pl.ds(2 * r, 2)] = add(
-            dbuf[pl.ds(2 * r, 2), :, span(y * quarter, eighth)], ya[pl.ds(2 * r, 2)]
-        )
-        xa_copy(r).start()
+            xb_copy(u, yq).start()
+
+    def stage_b(u):
+        r = u // pieces
+        ya_copy(u).wait_recv()
+        ya[pl.ds(2 * r, 2), half(u)] = add(
+            dbuf[pl.ds(2 * r, 2), half(u), span(y * quarter, eighth)],
+            ya[pl.ds(2 * r, 2), half(u)],
+        )
+        xa_copy(u).start()
         for yq in (0, 1):
-            xb_copy(r, yq).wait_recv()
+            xb_copy(u, yq).wait_recv()
             at = span(yq * eighth, eighth)
-            mine = dbuf[2 * r + x, :, span(yq * quarter + eighth, eighth)]
-            xb[r, :, at] = add(mine, xb[r, :, at])
-        yb_copy(r).start()
-
-    def stage_c(r):
-        xa_copy(r).wait_recv()
-        own[r, :, 0:eighth] = add(ya[2 * r + x], xa[r])
-        yb_copy(r).wait_recv()
-        own[r, :, eighth:quarter] = add(xb[r, :, span(y * eighth, eighth)], yb[r])
-
-    def stage_d(r):
-        @pl.when((z > 0) & (z <= r))
-        def _():
-            up_copy(r).wait_recv()
-            own[r] = add(own[r], rup[r])
-
-        @pl.when((z < nz - 1) & (z >= r))
-        def _():
-            dn_copy(r).wait_recv()
-            own[r] = add(own[r], rdn[r])
-
-        @pl.when(z < r)
-        def _():
-            up_copy(r).start()
-
-        @pl.when(z > r)
-        def _():
-            dn_copy(r).start()
-
-        @pl.when(z == r)
-        def _():
-            out_ref[...] = own[r]
+            mine = dbuf[2 * r + x, half(u), span(yq * quarter + eighth, eighth)]
+            xb[r, half(u), at] = add(mine, xb[r, half(u), at])
+        yb_copy(u).start()
+
+    def stage_c(u):
+        r = u // pieces
+        xa_copy(u).wait_recv()
+        own[r, half(u), 0:eighth] = add(ya[2 * r + x, half(u)], xa[r, half(u)])
+        yb_copy(u).wait_recv()
+        own[r, half(u), eighth:quarter] = add(
+            xb[r, half(u), span(y * eighth, eighth)], yb[r, half(u)]
+        )
+
+    def stage_d(u):
+        r = u // pieces
+
+        @pl.when(z != r)
+        def _():
+            z_copy(u, r).start()
 
     last_first = [nz - 1 - i // 2 if i % 2 == 0 else i // 2 for i in range(nz)]
     order = [[k] + [r for r in last_first if r != k] for k in range(nz)]
-    due = [[order[k].index(r) + 2 for r in range(nz)] for k in range(nz)]
-    for r in range(nz):
-        for k in range(1, r):
-            due[k][r] = max(due[k][r], due[k - 1][r] + 1)
-        for k in range(nz - 2, r, -1):
-            due[k][r] = max(due[k][r], due[k + 1][r] + 1)
-        for k in (r - 1, r + 1):
-            if 0 <= k < nz:
-                due[r][r] = max(due[r][r], due[k][r] + 1)
-    steps = max(max(line) for line in due) + 1
-
-    def row_of(i):
+    units = nz * pieces
+
+    def unit_of(i):
         row = z
         for k in range(nz):
             for j in range(1, nz):
-                row = jnp.where((z == k) & (i == j), order[k][j], row)
-        return row
+                row = jnp.where((z == k) & (i // pieces == j), order[k][j], row)
+        return row * pieces + i % pieces
 
     def step(i, carry):
-        @pl.when(i == 1)
+        @pl.when(i == pieces)
         def _():
             for s in range(1, nz):
                 at_distance(s, lambda row, way: from_y(2 * row + x))
@@ -381,39 +383,35 @@
                 at_distance(s, lambda row, way: arrived(2 * row + x))
                 at_distance(s, lambda row, way: arrived(2 * row + 1 - x))
 
-        @pl.when(i < nz)
-        def _():
-            compute(row_of(i))
-            stage_a(row_of(i))
-
-        @pl.when((i >= 1) & (i < nz + 1))
-        def _():
-            stage_b(row_of(i - 1))
-
-        @pl.when((i >= 2) & (i < nz + 2))
-        def _():
-            stage_c(row_of(i - 2))
-
-        def chain(r, inner):
-            when = 0
-            for k in range(nz):
-                for j in range(nz):
-                    when = jnp.where((z == k) & (r == j), due[k][j], when)
-
-            @pl.when(i == when)
-            def _():
-                stage_d(r)
-
-            return inner
-
-        lax.fori_loop(0, nz, chain, 0)
+        @pl.when(i < units)
+        def _():
+            compute(unit_of(i))
+            stage_a(unit_of(i))
+
+        @pl.when((i >= 1) & (i < units + 1))
+        def _():
+            stage_b(unit_of(i - 1))
+
+        @pl.when((i >= 2) & (i < units + 2))
+        def _():
+            stage_c(unit_of(i - 2))
+            stage_d(unit_of(i - 2))
+
         return carry
 
     from_y(2 * z + 1 - x)
     arrived(2 * z + 1 - x)
     for item in weight_copies:
         item.wait()
-    lax.fori_loop(0, steps, step, 0)
+    lax.fori_loop(0, units + 2, step, 0)
+
+    for p in range(pieces):
+        for k in range(1, nz):
+            z_wait(lax.rem(z + k, nz), p).wait_recv()
+        total = own[z, half(p)].astype(jnp.float32)
+        for k in range(1, nz):
+            total = total + zin[lax.rem(z + k, nz), half(p)].astype(jnp.float32)
+        out_ref[half(p), :] = total.astype(jnp.bfloat16)
 
     def sent(block, direction):
         for k in (0, 1, 2):
@@ -443,31 +441,28 @@
 
     others(passed)
 
-    def finish(r, carry):
+    def finish(u, carry):
         for yq in (0, 1):
-            d_copy(r, yq, 1 - c).wait_send()
-            xb_copy(r, yq).wait_send()
-        ya_copy(r).wait_send()
-        xa_copy(r).wait_send()
-        yb_copy(r).wait_send()
-
-        @pl.when(z < r)
-        def _():
-            up_copy(r).wait_send()
-
-        @pl.when(z > r)
-        def _():
-            dn_copy(r).wait_send()
+            d_copy(u, yq, 1 - c).wait_send()
+            xb_copy(u, yq).wait_send()
+        ya_copy(u).wait_send()
+        xa_copy(u).wait_send()
+        yb_copy(u).wait_send()
+
+        @pl.when(z != u // pieces)
+        def _():
+            z_copy(u, u // pieces).wait_send()
 
         return carry
 
-    lax.fori_loop(0, nz, finish, 0)
+    lax.fori_loop(0, units, finish, 0)
 
 
 def dense(tokens, norm_gain, expert_ids, route_weights, gate_weight, up_weight, down_weight):
     rows, width = tokens.shape
     n_ep = lax.axis_size("ep")
     nz = n_ep // 2
+    nu = nz * 2
     ff = gate_weight.shape[2]
     quarter = width // lax.axis_size("tp")
     eighth = quarter // 2
@@ -485,11 +480,11 @@
         scratch_shapes=[
             pltpu.VMEM((n_ep, rows, width), bf16),
             pltpu.VMEM((n_ep, n_ep, rows), jnp.float32),
-            pltpu.VMEM((2 * rows, 128), jnp.float32),
+            pltpu.VMEM((2 * rows // 2, 128), jnp.float32),
             pltpu.VMEM((width, ff), bf16),
             pltpu.VMEM((width, ff), bf16),
             pltpu.VMEM((ff, width), bf16),
-            pltpu.VMEM((2 * rows, ff), bf16),
+            pltpu.VMEM((2 * rows // 2, ff), bf16),
             pltpu.VMEM((n_ep, rows, width), bf16),
             pltpu.VMEM((n_ep, rows, 2 * quarter), bf16),
             pltpu.VMEM((n_ep, rows, eighth), bf16),
@@ -498,18 +493,17 @@
             pltpu.VMEM((nz, rows, eighth), bf16),
             pltpu.VMEM((nz, rows, quarter), bf16),
             pltpu.VMEM((nz, rows, quarter), bf16),
-            pltpu.VMEM((nz, rows, quarter), bf16),
             dma((3,)),
             dma((2, 3, n_ep)), dma((3, n_ep)),
             dma((3, n_ep)), dma((3, n_ep)),
             dma((n_ep,)), dma((n_ep,)),
             dma((3, n_ep)), dma((3, n_ep)),
-            dma((nz, 2)), dma((nz, 2)),
-            dma((nz,)), dma((nz,)),
-            dma((nz, 2)), dma((nz, 2)),
-            dma((nz,)), dma((nz,)),
-            dma((nz,)), dma((nz,)),
-            dma((2, nz)), dma((2, nz)),
+            dma((nu, 2)), dma((nu, 2)),
+            dma((nu,)), dma((nu,)),
+            dma((nu, 2)), dma((nu, 2)),
+            dma((nu,)), dma((nu,)),
+            dma((nu,)), dma((nu,)),
+            dma((nu,)), dma((nz, nu // nz)),
         ],
         compiler_params=pltpu.CompilerParams(
             collective_id=0, has_side_effects=True, vmem_limit_bytes=60 * 1024 * 1024

time: 105 us -> 101 us (0.962)
  Pallas kernels: 102 us -> 98.2 us
    pallas_call x1, Pallas kernels: 102 us -> 98.2 us  [dense(): pl.pallas_call(functools.partial(kernel, n_ep), out_shape=jax.ShapeDtypeS...]
where the time goes in v4:
time: 101 us
  Pallas kernels  98.2 us (97%)
  local copies, waits for them, and re-layouts  1.67 us (2%)
  other arithmetic  1.31 us (1%)
    pallas_call x1, Pallas kernels, dense(): pl.pallas_call(functools.partial(kernel, n_ep), out_shape=jax.ShapeDtypeS...  98.2 us

profile of v4, /device:TPU:8, one launch (start us, length us, event | category | flops | bytes accessed | tf_op | source)
XLA Modules:
  0.0 101.2 jit_solution(721035057963872357)
XLA Ops:
  0.0 1.3 %select_reduce_fusion = f32[256,8]{0,1:T(8,128)} fusion(f32[256,4]{0,1:T(4,128)} %param.10, s32[256,4]{0,1:T(4,128)} %param.9), kind=kLoop, calls=%fused_computation | loop fusion | flops 22528 | bytes 16384 | tf_op jit(solution)/shard_map/reduce_sum | solution.py:470
  1.3 98.2 %shard_map.73 = bf16[256,512]{1,0:T(8,128)(2,1)} custom-call(bf16[256,2048]{1,0:T(8,128)(2,1)} %tokens_ref.1, f32[1,2048]{1,0:T(1,128)} %bitcast.3, f32[8,256]{1,0:T(8,128)} %bitcast.2, bf16[1,2048,512]{2,1,0:T(8,128)(2,1)} %gate_hbm.1, bf16[1,2048,512]{2,1,0:T(8,128)(2,1)} %up_hbm.1, bf16[1,512,2048]{2,1,0:T(8,128)(2,1)} %down_hbm.1), custom_call_target="tpu_custom_call" | custom-call | tf_op jit(solution)/shard_map/pallas_call | solution.py:475
  99.5 1.7 %copy.11 = bf16[256,512]{1,0:T(8,128)(2,1)} copy(bf16[256,512]{1,0:T(8,128)(2,1)} %shard_map.73) | data formatting | bytes 524288
